TPU v7x, 32 devices: a whole 2x2x4 slice. The times are simulated.
32 devices in a mesh: fs: 16 (over z, y, x), tp: 2 (over core).
Axes of the slice: x: 2, y: 2, z: 4, core: 2. Of those that a mesh axis runs over, the one named last changes fastest.
Arguments:
- tokens: bfloat16 [4096, 2048], P('fs'), may hold values from -6 to 6
- routes: int32 [4096, 6], P('fs'), may hold values from 0 to 15, all different within a row; in each aligned block of 256 rows (0 to 255, 256 to 511, ...) at most 160 rows name the same one
- route_weights: float32 [4096, 6], P('fs'), may hold values from 0.1 to 1
- norm_gain: float32 [2048], P('fs'), may hold values from 0.1 to 1.9
- expert_gate: float32 [16, 2048, 1024], P(None, 'fs', 'tp'), may hold values from -0.125 to 0.125
- expert_up: float32 [16, 2048, 1024], P(None, 'fs', 'tp'), may hold values from -0.125 to 0.125
- expert_down: float32 [16, 2048, 1024], P(None, 'fs', 'tp'), may hold values from -0.1875 to 0.1875
- shared_gate: float32 [2048, 1024], P('fs', 'tp'), may hold values from -0.125 to 0.125
- shared_up: float32 [2048, 1024], P('fs', 'tp'), may hold values from -0.125 to 0.125
- shared_down: float32 [2048, 1024], P('fs', 'tp'), may hold values from -0.1875 to 0.1875
Outputs:
- layer_output: bfloat16 [4096, 2048], P('fs', 'tp')
- sample_gate: bfloat16 [16, 2048, 1024], P('fs', None, 'tp')
- sample_up: bfloat16 [16, 2048, 1024], P('fs', None, 'tp')
- sample_down: bfloat16 [16, 2048, 1024], P('fs', None, 'tp')
- common_gate: bfloat16 [2048, 1024], P(None, 'tp')
- common_up: bfloat16 [2048, 1024], P(None, 'tp')
- common_down: bfloat16 [2048, 1024], P(None, 'tp')
Inputs may be any that keep to these rules, and one draw needn't show every extreme that they name: `routes`: each row names 6 different experts. In each aligned block of 256 rows (the rows of one index of fs) no expert is named by more than 160 rows, a bound that some expert reaches in some blocks.
All inputs are finite; a program needn't handle non-finite values.
Results may differ from a plain program's by a relative error of at most 0.015.
Values may be sent and summed in bfloat16 or wider, within the bound.
A program may use at most 128 MiB of HBM per device.

v0:
```python
import jax
import jax.numpy as jnp
from jax import lax
from jax.sharding import PartitionSpec as P

EPSILON = 1e-06


def normalize(tokens):
    values = tokens.astype(jnp.float32)
    scale = lax.rsqrt(jnp.mean(values * values, axis=-1, keepdims=True) + EPSILON)
    return (values * scale).astype(jnp.bfloat16)


def slot_table(routes, experts, capacity):
    flat_route = routes.reshape(-1)
    member = (flat_route[:, None] == jnp.arange(experts, dtype=jnp.int32)[None, :]).astype(
        jnp.int32
    )
    before = jnp.sum((jnp.cumsum(member, axis=0) - member) * member, axis=1)
    return flat_route * capacity + before


def body(
    tokens,
    routes,
    route_weights,
    norm_gain,
    expert_gate,
    expert_up,
    expert_down,
    shared_gate,
    shared_up,
    shared_down,
):
    gain_rows = norm_gain[None, :, None]
    rounded = (
        (expert_gate * gain_rows).astype(jnp.bfloat16),
        (expert_up * gain_rows).astype(jnp.bfloat16),
        expert_down.astype(jnp.bfloat16),
    )
    sample_gate, sample_up, sample_down = (
        lax.all_to_all(rounded[0], "fs", split_axis=0, concat_axis=1, tiled=True),
        lax.all_to_all(rounded[1], "fs", split_axis=0, concat_axis=1, tiled=True),
        lax.all_to_all(rounded[2], "fs", split_axis=0, concat_axis=1, tiled=True),
    )
    gate_rows = sample_gate[0]
    up_rows = sample_up[0]
    down_rows = sample_down[0]
    normed = normalize(tokens)
    tok_rows, width = normed.shape
    picks = routes.shape[1]
    experts = expert_gate.shape[0]
    tp_count = lax.axis_size("tp")
    capacity = min(tok_rows, tp_count * max(1, tok_rows * picks * 5 // (3 * experts * tp_count)))
    slots = slot_table(routes, experts, capacity)
    sources = (
        jnp.full((experts * capacity,), tok_rows, jnp.int32)
        .at[slots]
        .set(jnp.arange(tok_rows * picks, dtype=jnp.int32) // picks)
    )
    padded = jnp.concatenate([normed, jnp.zeros((1, width), jnp.bfloat16)], axis=0)
    outgoing = padded[sources].reshape(experts, capacity, width)
    shared_rounded = (
        (shared_gate * norm_gain[:, None]).astype(jnp.bfloat16),
        (shared_up * norm_gain[:, None]).astype(jnp.bfloat16),
        shared_down.astype(jnp.bfloat16),
    )
    common_gate, common_up, common_down = (
        lax.all_gather(shared_rounded[0], "fs", axis=0, tiled=True),
        lax.all_gather(shared_rounded[1], "fs", axis=0, tiled=True),
        lax.all_gather(shared_rounded[2], "fs", axis=0, tiled=True),
    )
    shared_gate_act = jnp.dot(normed, common_gate, preferred_element_type=jnp.float32)
    shared_up_act = jnp.dot(normed, common_up, preferred_element_type=jnp.float32)
    shared_hidden = (jax.nn.silu(shared_gate_act) * shared_up_act).astype(jnp.bfloat16)
    shared_terms = jnp.einsum(
        "th,dh->td", shared_hidden, common_down, preferred_element_type=jnp.float32
    )
    share = capacity // tp_count
    whole_gate, whole_up, whole_down = (
        lax.all_gather(gate_rows, "tp", axis=1, tiled=True),
        lax.all_gather(up_rows, "tp", axis=1, tiled=True),
        lax.all_gather(down_rows, "tp", axis=1, tiled=True),
    )
    own_share = lax.dynamic_slice_in_dim(outgoing, lax.axis_index("tp") * share, share, 1)
    block = lax.all_to_all(own_share, "fs", split_axis=0, concat_axis=0, tiled=True)
    flat = block.reshape(-1, width)
    gate = jnp.dot(flat, whole_gate, preferred_element_type=jnp.float32)
    upward = jnp.dot(flat, whole_up, preferred_element_type=jnp.float32)
    hidden = (jax.nn.silu(gate) * upward).astype(jnp.bfloat16)
    parts = jnp.einsum(
        "rbf,dbf->rbd",
        hidden.reshape(flat.shape[0], tp_count, -1),
        whole_down.reshape(width, tp_count, -1),
        preferred_element_type=jnp.float32,
    ).astype(jnp.bfloat16)
    parts = lax.optimization_barrier(parts)
    total = jnp.sum(parts.astype(jnp.float32), axis=1).astype(jnp.bfloat16)
    results = total.reshape(block.shape[0], block.shape[1], width)
    back = lax.all_to_all(results, "fs", split_axis=0, concat_axis=0, tiled=True).reshape(
        experts * share, width
    )
    position = slots % capacity
    owner = position // share
    local = slots // capacity * share + position % share
    taken = back[local].astype(jnp.float32).reshape(tok_rows, picks, width)
    keep = (owner == lax.axis_index("tp")).astype(jnp.float32).reshape(tok_rows, picks)
    routed_part = jnp.sum(taken * (route_weights * keep)[:, :, None], axis=1)
    shared_part = lax.optimization_barrier(shared_terms.astype(jnp.bfloat16)).astype(jnp.float32)
    layer_output = lax.psum_scatter(
        (routed_part + shared_part).astype(jnp.bfloat16), "tp", scatter_dimension=1, tiled=True
    )
    return (layer_output, sample_gate, sample_up, sample_down, common_gate, common_up, common_down)


def solution(mesh):
    return jax.shard_map(
        body,
        mesh=mesh,
        in_specs=(
            P("fs", None),
            P("fs", None),
            P("fs", None),
            P("fs"),
            P(None, "fs", "tp"),
            P(None, "fs", "tp"),
            P(None, "fs", "tp"),
            P("fs", "tp"),
            P("fs", "tp"),
            P("fs", "tp"),
        ),
        out_specs=(
            P("fs", "tp"),
            P("fs", None, "tp"),
            P("fs", None, "tp"),
            P("fs", None, "tp"),
            P(None, "tp"),
            P(None, "tp"),
            P(None, "tp"),
        ),
        check_vma=False,
    )
```

profile of v0, /device:TPU:0, one launch (start us, length us, event | category | flops | bytes accessed | tf_op | source)
XLA Modules:
  0.0 618.7 jit_solution(1220370238295980275)
XLA Ops:
  7.2 6.1 multiply_convert_fusion.1
  13.3 57.0 %all_to_all.46 = bf16[16,128,512]{2,1,0:T(8,128)(2,1)} all-to-all(bf16[16,128,512]{2,1,0:T(8,128)(2,1)S(1)} %get-tuple-element.12), channel_id=1, replica_groups=mesh['fs'=16,'tp'=2] {'fs'}, dimensions={0} | all-to-all | bytes 4194304 | tf_op jit(solution)/shard_map/all_to_all | solution.py:43
  70.3 3.9 all-to-all-start.2
  74.3 3.8 convert_element_type.70
  78.1 38.7 %all-to-all-done.2 = bf16[16,128,512]{2,1,0:T(8,128)(2,1)S(1)} async-done(((bf16[16,128,512]{2,1,0:T(8,128)(2,1)}), bf16[16,128,512]{2,1,0:T(8,128)(2,1)S(1)}, u32[]{:S(2)}, u32[]{:S(2)}) %all-to-all-start.2) | async-done | bytes 2097184 | tf_op jit(solution)/shard_map/all_to_all | solution.py:44
  116.8 9.9 %all-to-all-start.3 = ((bf16[16,128,512]{2,1,0:T(8,128)(2,1)}), bf16[16,128,512]{2,1,0:T(8,128)(2,1)}, u32[]{:S(2)}, u32[]{:S(2)}) async-start(bf16[16,128,512]{2,1,0:T(8,128)(2,1)} %convert_element_type.70), calls=%async_computation.3 | async-start | bytes 4194304 | tf_op jit(solution)/shard_map/all_to_all | solution.py:45
  126.9 0.1 eq.39
  127.2 0.2 all-gather.7.cloned.1.call-update
  127.5 4.6 reduce-window.6
  132.0 0.4 slice_reduce_fusion
  132.5 0.2 reduce-window.9
  132.6 0.1 copy.29
  132.8 0.1 mul.113
  132.9 0.3 fusion.1
  133.2 0.2 fusion.2
  133.9 6.2 %scatter_custom_fusion = s32[2560]{0:T(1024)S(1)} fusion(s32[1536]{0:T(1024)S(1)} %get-tuple-element.8, s32[1536]{0:T(1024)S(1)} %add_select_fusion.2, s32[]{:T(128)} %constant.63.clone.1), kind=kCustom, calls=%fused_computation.62 | custom fusion | bytes 10244 | tf_op jit(solution)/shard_map/scatter | solution.py:60
  140.1 10.8 %gather_fusion = bf16[2560,2048]{1,0:T(8,128)(2,1)} fusion(bf16[257,2048]{1,0:T(8,128)(2,1)S(1)} %concatenate.3, s32[3072]{0:T(1024)S(1)} %pad_clamp_fusion), kind=kCustom, calls=%fused_computation | custom fusion | bytes 20981760 | tf_op jit(solution)/shard_map/gather | solution.py:63
  150.9 5.7 constant_dynamic-slice_fusion
  156.6 12.7 %all-to-all-done.3 = bf16[16,128,512]{2,1,0:T(8,128)(2,1)} async-done(((bf16[16,128,512]{2,1,0:T(8,128)(2,1)}), bf16[16,128,512]{2,1,0:T(8,128)(2,1)}, u32[]{:S(2)}, u32[]{:S(2)}) %all-to-all-start.3) | async-done | bytes 2097184 | tf_op jit(solution)/shard_map/all_to_all | solution.py:45
  169.3 9.8 %all-to-all-start = ((bf16[16,80,2048]{2,1,0:T(8,128)(2,1)}), bf16[16,80,2048]{2,1,0:T(8,128)(2,1)}, u32[]{:S(2)}, u32[]{:S(2)}) async-start(bf16[16,80,2048]{2,1,0:T(8,128)(2,1)} %constant_dynamic-slice_fusion), calls=%async_computation | async-start | bytes 10485760 | tf_op jit(solution)/shard_map/all_to_all | solution.py:87
  179.3 0.7 all-gather.9.cloned.1.call-update
  180.0 3.9 copy.39
  183.9 0.2 all-gather.13.cloned.1.call-start
  184.2 0.8 multiply_convert_fusion.4
  185.0 99.7 %all-to-all-done = bf16[16,80,2048]{2,1,0:T(8,128)(2,1)} async-done(((bf16[16,80,2048]{2,1,0:T(8,128)(2,1)}), bf16[16,80,2048]{2,1,0:T(8,128)(2,1)}, u32[]{:S(2)}, u32[]{:S(2)}) %all-to-all-start) | async-done | bytes 5242912 | tf_op jit(solution)/shard_map/all_to_all | solution.py:87
  284.7 10.6 %fusion.27 = f32[1280,1024]{0,1:T(8,128)} fusion(bf16[1280,2048]{1,0:T(8,128)(2,1)} %bitcast.2, bf16[2048,1024]{1,0:T(8,128)(2,1)} %all-gather.7.cloned.1.call-done), kind=kOutput, calls=%fused_computation.68 | convolution fusion | flops 5368709120 | bytes 14680064 | tf_op jit(solution)/shard_map/dot_general | solution.py:89
  295.3 11.6 %multiply_convert_fusion = bf16[1280,1024]{0,1:T(8,128)(2,1)} fusion(f32[1280,1024]{0,1:T(8,128)} %fusion.27, bf16[1280,2048]{1,0:T(8,128)(2,1)} %bitcast.2, bf16[2048,1024]{1,0:T(8,128)(2,1)} %all-gather.9.cloned.1.call-done), kind=kOutput, calls=%fused_computation.6 | convolution fusion | flops 5376573440 | bytes 17301504 | tf_op jit(solution)/shard_map/dot_general | solution.py:90
  306.9 10.9 %fusion = bf16[1280,2,2048]{2,0,1:T(8,128)(2,1)} fusion(bf16[1280,2,512]{0,2,1:T(8,128)(2,1)} %bitcast.52, bf16[2048,2,512]{0,2,1:T(8,128)(2,1)} %bitcast.51), kind=kOutput, calls=%fused_computation.5 | convolution fusion | flops 5373952000 | bytes 17301504 | tf_op jit(solution)/shard_map/rbf,dbf->rbd/dot_general | solution.py:92
  317.8 11.2 %reduce_sum.46 = bf16[1280,2048]{1,0:T(8,128)(2,1)} reduce(bf16[1280,2,2048]{2,0,1:T(8,128)(2,1)} %fusion, bf16[]{:T(256)} %constant.62.clone.1), dimensions={1}, to_apply=%region_5.6 | reduce | flops 2621440 | bytes 15728642 | tf_op jit(solution)/shard_map/reduce_sum | solution.py:99
  329.0 35.7 %all-to-all-start.4 = ((bf16[16,80,2048]{2,1,0:T(8,128)(2,1)}), bf16[16,80,2048]{2,1,0:T(8,128)(2,1)}, u32[]{:S(2)}, u32[]{:S(2)}) async-start(bf16[16,80,2048]{2,1,0:T(8,128)(2,1)} %bitcast.44), calls=%async_computation.4 | async-start | bytes 10485760 | tf_op jit(solution)/shard_map/all_to_all | solution.py:101
  364.8 0.5 all-gather.15.cloned.1.call-update
  365.4 0.7 convert_element_type.78
  366.6 2.3 fusion.28
  368.9 120.3 %all-gather.15.cloned.1.call-done = bf16[2048,512]{1,0:T(8,128)(2,1)} async-done(((bf16[128,512]{1,0:T(8,128)(2,1)}), bf16[2048,512]{1,0:T(8,128)(2,1)}) %all-gather.15.cloned.1.call-update) | async-done | bytes 2097168 | tf_op jit(solution)/shard_map/all_gather | solution.py:71
  489.2 62.3 %all-gather.17.cloned.1.call-done = bf16[2048,512]{1,0:T(8,128)(2,1)} async-done(((bf16[128,512]{1,0:T(8,128)(2,1)}), bf16[2048,512]{1,0:T(8,128)(2,1)}) %all-gather.17.cloned.1.call-update) | async-done | bytes 2097168 | tf_op jit(solution)/shard_map/all_gather | solution.py:72
  551.5 3.6 convolution_convert_fusion.1
  555.1 16.1 %gather_fusion.1 = bf16[1536,2048]{1,0:T(8,128)(2,1)} fusion(bf16[1280,2048]{1,0:T(8,128)(2,1)} %bitcast.10, s32[2048]{0:T(1024)S(1)} %pad_clamp_fusion.1), kind=kCustom, calls=%fused_computation.1 | custom fusion | bytes 12589056 | tf_op jit(solution)/shard_map/gather | solution.py:107
  571.2 11.7 %reshape.194 = f32[256,6,2048]{2,1,0:T(8,128)} reshape(bf16[1536,2048]{1,0:T(8,128)(2,1)} %gather_fusion.1) | data formatting | bytes 18874368 | tf_op jit(solution)/shard_map/convert_element_type | solution.py:107
  582.9 9.4 %multiply_reduce_fusion = f32[256,2048]{1,0:T(8,128)S(1)} fusion(f32[256,6,2048]{2,1,0:T(8,128)} %reshape.194, f32[256,6]{1,0:T(8,128)S(1)} %copy.36), kind=kLoop, calls=%fused_computation.3 | loop fusion | flops 5767168 | bytes 14686208 | tf_op jit(solution)/shard_map/reduce_sum | solution.py:109
  592.3 1.3 add_convert_fusion
  593.7 7.3 %reduce-scatter.2.cloned.1.call-done = bf16[256,1024]{1,0:T(8,128)(2,1)} async-done(((bf16[256,2048]{1,0:T(8,128)(2,1)}), bf16[256,1024]{1,0:T(8,128)(2,1)}) %reduce-scatter.2.cloned.1.call-update) | async-done | bytes 524304 | tf_op jit(solution)/shard_map/reduce_scatter | solution.py:111
  601.0 1.3 copy.48
  602.3 1.0 copy-done.2
  603.4 1.3 copy.49
  604.7 3.2 copy.50
  607.9 1.3 copy.51
  609.2 1.3 copy.52
  610.5 1.3 copy.53
  (57 shorter events, 1.5 us)
Async XLA Ops:
  70.3 46.5 %all-to-all-start.2 = ((bf16[16,128,512]{2,1,0:T(8,128)(2,1)}), bf16[16,128,512]{2,1,0:T(8,128)(2,1)S(1)}, u32[]{:S(2)}, u32[]{:S(2)}) async-start(bf16[16,128,512]{2,1,0:T(8,128)(2,1)} %get-tuple-element.11), calls=%async_computation.2 | async-start | bytes 4194304 | tf_op jit(solution)/shard_map/all_to_all | solution.py:44
  74.3 52.5 %copy-start.10 = (s32[256,6]{0,1:T(8,128)S(1)}, s32[256,6]{0,1:T(8,128)}, u32[]{:S(2)}) copy-start(s32[256,6]{0,1:T(8,128)} %param.11) | copy-start | bytes 18436
  78.1 54.8 %copy-start.3 = (bf16[256,2048]{1,0:T(8,128)(2,1)S(1)}, bf16[256,2048]{1,0:T(8,128)(2,1)}, u32[]{:S(2)}) copy-start(bf16[256,2048]{1,0:T(8,128)(2,1)} %param.10) | copy-start | bytes 3145732
  116.8 16.4 %copy-start.1 = (bf16[16,128,512]{2,1,0:T(8,128)(2,1)}, bf16[16,128,512]{2,1,0:T(8,128)(2,1)S(1)}, u32[]{:S(2)}) copy-start(bf16[16,128,512]{2,1,0:T(8,128)(2,1)S(1)} %all-to-all-done.2) | copy-start | bytes 6291460
  116.8 52.5 %all-to-all-start.3 = ((bf16[16,128,512]{2,1,0:T(8,128)(2,1)}), bf16[16,128,512]{2,1,0:T(8,128)(2,1)}, u32[]{:S(2)}, u32[]{:S(2)}) async-start(bf16[16,128,512]{2,1,0:T(8,128)(2,1)} %convert_element_type.70), calls=%async_computation.3 | async-start | bytes 4194304 | tf_op jit(solution)/shard_map/all_to_all | solution.py:45
  126.7 58.3 %all-gather.7.cloned.1.call-start = ((), (), s32[]{:S(2)}) async-start(), calls=%async_computation.6 | async-start | bytes 6291456 | tf_op jit(solution)/shard_map/all_gather | solution.py:82
  169.3 115.4 %all-to-all-start = ((bf16[16,80,2048]{2,1,0:T(8,128)(2,1)}), bf16[16,80,2048]{2,1,0:T(8,128)(2,1)}, u32[]{:S(2)}, u32[]{:S(2)}) async-start(bf16[16,80,2048]{2,1,0:T(8,128)(2,1)} %constant_dynamic-slice_fusion), calls=%async_computation | async-start | bytes 10485760 | tf_op jit(solution)/shard_map/all_to_all | solution.py:87
  179.2 116.1 %all-gather.9.cloned.1.call-start = ((), (), s32[]{:S(2)}) async-start(), calls=%async_computation.7 | async-start | bytes 6291456 | tf_op jit(solution)/shard_map/all_gather | solution.py:83
  179.2 4.9 copy-start.8
  179.2 4.9 copy-start.9
  179.2 4.9 copy-start.12
  179.9 126.9 %all-gather.11.cloned.1.call-start = ((), (), s32[]{:S(2)}) async-start(), calls=%async_computation.8 | async-start | bytes 6291456 | tf_op jit(solution)/shard_map/all_gather | solution.py:84
  183.9 182.7 %all-gather.13.cloned.1.call-start = ((), (), s32[]{:S(2)}) async-start(), calls=%async_computation.9 | async-start | bytes 2228224 | tf_op jit(solution)/shard_map/all_gather | solution.py:70
  329.0 36.4 %copy-start.7 = (f32[128,512]{1,0:T(8,128)S(1)}, f32[128,512]{1,0:T(8,128)}, u32[]{:S(2)}) copy-start(f32[128,512]{1,0:T(8,128)} %param.19) | copy-start | bytes 786436
  329.0 37.4 %copy-start.11 = (f32[256,6]{0,1:T(8,128)S(1)}, f32[256,6]{0,1:T(8,128)}, u32[]{:S(2)}) copy-start(f32[256,6]{0,1:T(8,128)} %param.12) | copy-start | bytes 18436
  329.0 226.1 %all-to-all-start.4 = ((bf16[16,80,2048]{2,1,0:T(8,128)(2,1)}), bf16[16,80,2048]{2,1,0:T(8,128)(2,1)}, u32[]{:S(2)}, u32[]{:S(2)}) async-start(bf16[16,80,2048]{2,1,0:T(8,128)(2,1)} %bitcast.44), calls=%async_computation.4 | async-start | bytes 10485760 | tf_op jit(solution)/shard_map/all_to_all | solution.py:101
  364.8 124.4 %all-gather.15.cloned.1.call-start = ((), (), s32[]{:S(2)}) async-start(), calls=%async_computation.10 | async-start | bytes 2228224 | tf_op jit(solution)/shard_map/all_gather | solution.py:71
  365.4 186.1 %all-gather.17.cloned.1.call-start = ((), (), s32[]{:S(2)}) async-start(), calls=%async_computation.11 | async-start | bytes 2228224 | tf_op jit(solution)/shard_map/all_gather | solution.py:72
  366.1 234.9 %reduce-scatter.2.cloned.1.call-start = ((), (), s32[]{:S(2)}) async-start(), calls=%async_computation.12 | async-start | bytes 1572864 | tf_op jit(solution)/shard_map/reduce_scatter | solution.py:111
  592.3 8.7 %copy-start = (bf16[16,128,512]{2,1,0:T(8,128)(2,1)S(1)}, bf16[16,128,512]{2,1,0:T(8,128)(2,1)}, u32[]{:S(2)}) copy-start(bf16[16,128,512]{2,1,0:T(8,128)(2,1)} %all_to_all.46) | copy-start | bytes 6291460
  601.0 2.3 copy-start.2
  603.4 4.5 copy-start.4
  604.7 4.5 copy-start.5
  607.9 2.6 copy-start.6
Sparse Core Ops, SparseCore 0:
  129.1 14.9 all-gather.6
  182.1 14.8 all-gather.8
  199.2 14.8 all-gather.10
  217.2 96.2 all-gather.12
  368.6 120.5 all-gather.14
  492.4 59.0 all-gather.16
  593.8 7.1 reduce-scatter.1
where the time goes:
time: 620 us; the launch traced here: 619 us
  waiting for transfers between devices  343 us (55%)
  local copies, waits for them, and re-layouts  66.9 us (11%)
  starting transfers between devices  59.8 us (10%)
  blocking collectives  57 us (9%)
  matrix products  39 us (6%)
  other arithmetic  38.9 us (6%)
  between operations  14.5 us (2%)
    all_gather x1, waiting for transfers between devices, body(): lax.all_gather(shared_rounded[1], 'fs', axis=0, tiled=True)  120 us
    all_to_all x1, waiting for transfers between devices, body(): lax.all_to_all(own_share, 'fs', split_axis=0, concat_axis=0, tiled=True)  99.7 us
    all_gather x1, waiting for transfers between devices, body(): lax.all_gather(shared_rounded[2], 'fs', axis=0, tiled=True)  62.3 us
    all_to_all x1, blocking collectives, body(): lax.all_to_all(rounded[0], 'fs', split_axis=0, concat_axis=1, tiled=True)  57 us
    all_to_all x1, waiting for transfers between devices, body(): lax.all_to_all(rounded[1], 'fs', split_axis=0, concat_axis=1, tiled=True)  38.7 us
    all_to_all x1, starting transfers between devices, body(): lax.all_to_all(results, 'fs', split_axis=0, concat_axis=0, tiled=True)  35.7 us
    gather x1, local copies, waits for them, and re-layouts, body(): taken = back[local].astype(jnp.float32).reshape(tok_rows, picks, width)  16.1 us
    all_to_all x1, waiting for transfers between devices, body(): lax.all_to_all(rounded[2], 'fs', split_axis=0, concat_axis=1, tiled=True)  12.7 us
  transfers between devices with their start and end apart: 11, of which 6 were waited for; matrix products, arithmetic and copies ran while one was open for 14% of the time, Pallas kernels for 0%

commit v1 on v0

--- a/solution.py
+++ b/solution.py
@@ -1,9 +1,31 @@
+import functools
 import jax
 import jax.numpy as jnp
 from jax import lax
 from jax.sharding import PartitionSpec as P
 
 EPSILON = 1e-06
+
+
+def _find_points(array_in, axis_tag, dim_i):
+    n_shards = lax.psum(1, axis_name=axis_tag)
+    rack = tuple(((kk, (kk + 1) % n_shards) for kk in range(n_shards)))
+    copies = tuple(((kk, (kk - 1) % n_shards) for kk in range(n_shards)))
+    y2, outcome_arr = ([array_in], [array_in])
+    for _ in range(n_shards // 2):
+        earlier = lax.ppermute(y2[-1], axis_name=axis_tag, perm=rack)
+        y2.append(earlier)
+    k0 = 0
+    while k0 < (n_shards - 1) // 2:
+        h_now = lax.ppermute(outcome_arr[-1], axis_name=axis_tag, perm=copies)
+        outcome_arr.append(h_now)
+        k0 += 1
+    a_now = jnp.concatenate([*y2[::-1], *outcome_arr[1:]], axis=dim_i)
+    t1 = lax.axis_index(axis_tag)
+    return jnp.roll(a_now, (t1 - n_shards // 2) * array_in.shape[dim_i], axis=dim_i)
+
+
+arrange_circles_now = functools.partial(_find_points, axis_tag="fs", dim_i=0)
 
 
 def normalize(tokens):
@@ -68,7 +90,7 @@
     )
     common_gate, common_up, common_down = (
         lax.all_gather(shared_rounded[0], "fs", axis=0, tiled=True),
-        lax.all_gather(shared_rounded[1], "fs", axis=0, tiled=True),
+        arrange_circles_now(shared_rounded[1]),
         lax.all_gather(shared_rounded[2], "fs", axis=0, tiled=True),
     )
     shared_gate_act = jnp.dot(normed, common_gate, preferred_element_type=jnp.float32)

time: 620 us -> 644 us (1.039)
  starting transfers between devices: 59.8 us -> 95.5 us
  waiting for transfers between devices: 343 us -> 329 us
    ppermute x0 -> x15, waiting for transfers between devices: none -> 127 us  [the longest x8 112 us: _find_points(): earlier = lax.ppermute(y2[-1], axis_name=axis_tag, perm=rack)]
    all_gather x1 -> x0, waiting for transfers between devices: 120 us -> none  [body(): lax.all_gather(shared_rounded[1], 'fs', axis=0, tiled=True)]
    ppermute x0 -> x15, starting transfers between devices: none -> 47.2 us  [the longest x7 42.7 us: _find_points(): h_now = lax.ppermute(outcome_arr[-1], axis_name=axis_tag, perm=copies)]
    all_to_all x1, waiting for transfers between devices: 99.7 us -> 80 us  [body(): lax.all_to_all(own_share, 'fs', split_axis=0, concat_axis=0, tiled=True)]
    all_gather x1, waiting for transfers between devices: 62.3 us -> 50.5 us  [body(): lax.all_gather(shared_rounded[2], 'fs', axis=0, tiled=True)]
    all_gather x1, waiting for transfers between devices: 0.02 us -> 11.6 us  [body(): lax.all_gather(gate_rows, 'tp', axis=1, tiled=True)]
    all_to_all x1, starting transfers between devices: 35.7 us -> 24.3 us  [body(): lax.all_to_all(results, 'fs', split_axis=0, concat_axis=0, tiled=True)]
  transfers between devices with their start and end apart: 11 -> 25, of which waited for: 6 -> 17; matrix products, arithmetic and copies ran while one was open for 14% -> 11% of each run, Pallas kernels for 0% -> 0%
where the time goes in v1:
time: 644 us; the launch traced here: 643 us
  waiting for transfers between devices  329 us (51%)
  starting transfers between devices  95.5 us (15%)
  local copies, waits for them, and re-layouts  67.7 us (11%)
  blocking collectives  57 us (9%)
  other arithmetic  38.9 us (6%)
  matrix products  38.9 us (6%)
  between operations  15.9 us (2%)
    ppermute x8, waiting for transfers between devices, _find_points(): earlier = lax.ppermute(y2[-1], axis_name=axis_tag, perm=rack)  112 us
    all_to_all x1, waiting for transfers between devices, body(): lax.all_to_all(own_share, 'fs', split_axis=0, concat_axis=0, tiled=True)  80 us
    all_to_all x1, blocking collectives, body(): lax.all_to_all(rounded[0], 'fs', split_axis=0, concat_axis=1, tiled=True)  57 us
    all_gather x1, waiting for transfers between devices, body(): lax.all_gather(shared_rounded[2], 'fs', axis=0, tiled=True)  50.5 us
    ppermute x7, starting transfers between devices, _find_points(): h_now = lax.ppermute(outcome_arr[-1], axis_name=axis_tag, perm=copies)  42.7 us
    all_to_all x1, waiting for transfers between devices, body(): lax.all_to_all(rounded[1], 'fs', split_axis=0, concat_axis=1, tiled=True)  38.7 us
    all_to_all x1, starting transfers between devices, body(): lax.all_to_all(results, 'fs', split_axis=0, concat_axis=0, tiled=True)  24.3 us
    gather x1, local copies, waits for them, and re-layouts, body(): taken = back[local].astype(jnp.float32).reshape(tok_rows, picks, width)  16.1 us
  transfers between devices with their start and end apart: 25, of which 17 were waited for; matrix products, arithmetic and copies ran while one was open for 11% of the time, Pallas kernels for 0%

profile of v1, /device:TPU:0, one launch (start us, length us, event | category | flops | bytes accessed | tf_op | source)
XLA Modules:
  0.0 642.5 jit_solution(8065882567579183464)
XLA Ops:
  8.0 6.1 multiply_convert_fusion.1
  14.1 57.0 %all_to_all.46 = bf16[16,128,512]{2,1,0:T(8,128)(2,1)} all-to-all(bf16[16,128,512]{2,1,0:T(8,128)(2,1)S(1)} %get-tuple-element.12), channel_id=1, replica_groups=mesh['fs'=16,'tp'=2] {'fs'}, dimensions={0} | all-to-all | bytes 4194304 | tf_op jit(solution)/shard_map/all_to_all | solution.py:65
  71.2 3.9 all-to-all-start.2
  75.1 3.8 convert_element_type.70
  78.9 38.7 %all-to-all-done.2 = bf16[16,128,512]{2,1,0:T(8,128)(2,1)S(1)} async-done(((bf16[16,128,512]{2,1,0:T(8,128)(2,1)}), bf16[16,128,512]{2,1,0:T(8,128)(2,1)S(1)}, u32[]{:S(2)}, u32[]{:S(2)}) %all-to-all-start.2) | async-done | bytes 2097184 | tf_op jit(solution)/shard_map/all_to_all | solution.py:66
  117.7 9.9 %all-to-all-start.3 = ((bf16[16,128,512]{2,1,0:T(8,128)(2,1)}), bf16[16,128,512]{2,1,0:T(8,128)(2,1)}, u32[]{:S(2)}, u32[]{:S(2)}) async-start(bf16[16,128,512]{2,1,0:T(8,128)(2,1)} %convert_element_type.70), calls=%async_computation.3 | async-start | bytes 4194304 | tf_op jit(solution)/shard_map/all_to_all | solution.py:67
  128.3 4.5 reduce-window.6
  135.3 6.2 scatter_custom_fusion
  141.5 10.9 %gather_fusion = bf16[2560,2048]{1,0:T(8,128)(2,1)} fusion(bf16[257,2048]{1,0:T(8,128)(2,1)S(1)} %concatenate.9, s32[3072]{0:T(1024)S(1)} %pad_clamp_fusion), kind=kCustom, calls=%fused_computation | custom fusion | bytes 20981760 | tf_op jit(solution)/shard_map/gather | solution.py:85
  152.4 5.7 constant_dynamic-slice_fusion.1
  158.1 12.1 %all-to-all-done.3 = bf16[16,128,512]{2,1,0:T(8,128)(2,1)} async-done(((bf16[16,128,512]{2,1,0:T(8,128)(2,1)}), bf16[16,128,512]{2,1,0:T(8,128)(2,1)}, u32[]{:S(2)}, u32[]{:S(2)}) %all-to-all-start.3) | async-done | bytes 2097184 | tf_op jit(solution)/shard_map/all_to_all | solution.py:67
  170.2 9.8 %all-to-all-start = ((bf16[16,80,2048]{2,1,0:T(8,128)(2,1)}), bf16[16,80,2048]{2,1,0:T(8,128)(2,1)}, u32[]{:S(2)}, u32[]{:S(2)}) async-start(bf16[16,80,2048]{2,1,0:T(8,128)(2,1)} %constant_dynamic-slice_fusion.1), calls=%async_computation | async-start | bytes 10485760 | tf_op jit(solution)/shard_map/all_to_all | solution.py:109
  181.7 3.9 copy.39
  185.7 11.6 %all-gather.6.cloned.1.call-done = bf16[2048,1024]{1,0:T(8,128)(2,1)} async-done(((bf16[2048,512]{1,0:T(8,128)(2,1)}), bf16[2048,1024]{1,0:T(8,128)(2,1)}) %all-gather.6.cloned.1.call-update) | async-done | bytes 4194320 | tf_op jit(solution)/shard_map/all_gather | solution.py:104
  197.3 80.0 %all-to-all-done = bf16[16,80,2048]{2,1,0:T(8,128)(2,1)} async-done(((bf16[16,80,2048]{2,1,0:T(8,128)(2,1)}), bf16[16,80,2048]{2,1,0:T(8,128)(2,1)}, u32[]{:S(2)}, u32[]{:S(2)}) %all-to-all-start) | async-done | bytes 5242912 | tf_op jit(solution)/shard_map/all_to_all | solution.py:109
  277.3 10.6 %fusion.27 = f32[1280,1024]{0,1:T(8,128)} fusion(bf16[1280,2048]{1,0:T(8,128)(2,1)} %bitcast.2, bf16[2048,1024]{1,0:T(8,128)(2,1)} %all-gather.6.cloned.1.call-done), kind=kOutput, calls=%fused_computation.101 | convolution fusion | flops 5368709120 | bytes 14680064 | tf_op jit(solution)/shard_map/dot_general | solution.py:111
  287.9 10.4 %multiply_convert_fusion = bf16[1280,1024]{0,1:T(8,128)(2,1)S(1)} fusion(f32[1280,1024]{0,1:T(8,128)} %fusion.27, bf16[1280,2048]{1,0:T(8,128)(2,1)} %bitcast.2, bf16[2048,1024]{1,0:T(8,128)(2,1)} %all-gather.8.cloned.1.call-done), kind=kOutput, calls=%fused_computation.6 | convolution fusion | flops 5376573440 | bytes 17301504 | tf_op jit(solution)/shard_map/dot_general | solution.py:112
  298.4 10.6 %fusion = bf16[1280,2,2048]{2,0,1:T(8,128)(2,1)} fusion(bf16[1280,2,512]{0,2,1:T(8,128)(2,1)S(1)} %bitcast.52, bf16[2048,2,512]{0,2,1:T(8,128)(2,1)} %bitcast.51), kind=kOutput, calls=%fused_computation.5 | convolution fusion | flops 5373952000 | bytes 17301504 | tf_op jit(solution)/shard_map/rbf,dbf->rbd/dot_general | solution.py:114
  309.0 11.2 %reduce_sum.46 = bf16[1280,2048]{1,0:T(8,128)(2,1)} reduce(bf16[1280,2,2048]{2,0,1:T(8,128)(2,1)} %fusion, bf16[]{:T(256)} %constant.86.clone.1), dimensions={1}, to_apply=%region_5.6 | reduce | flops 2621440 | bytes 15728642 | tf_op jit(solution)/shard_map/reduce_sum | solution.py:121
  320.2 24.3 %all-to-all-start.4 = ((bf16[16,80,2048]{2,1,0:T(8,128)(2,1)}), bf16[16,80,2048]{2,1,0:T(8,128)(2,1)}, u32[]{:S(2)}, u32[]{:S(2)}) async-start(bf16[16,80,2048]{2,1,0:T(8,128)(2,1)} %bitcast.44), calls=%async_computation.4 | async-start | bytes 10485760 | tf_op jit(solution)/shard_map/all_to_all | solution.py:123
  345.4 1.9 collective-permute-start
  347.3 99.3 %collective-permute-done = bf16[128,512]{1,0:T(8,128)(2,1)S(1)} collective-permute-done((bf16[128,512]{1,0:T(8,128)(2,1)S(1)}, bf16[128,512]{1,0:T(8,128)(2,1)S(1)}, u32[]{:S(2)}, u32[]{:S(2)}) %collective-permute-start) | collective-permute-done | bytes 131104 | tf_op jit(solution)/shard_map/ppermute | solution.py:16
  446.6 5.6 collective-permute-start.8
  452.2 5.9 collective-permute-done.1
  458.1 2.5 collective-permute-start.2
  460.6 8.7 %collective-permute-start.9 = (bf16[128,512]{1,0:T(8,128)(2,1)S(1)}, bf16[128,512]{1,0:T(8,128)(2,1)S(1)}, u32[]{:S(2)}, u32[]{:S(2)}) collective-permute-start(bf16[128,512]{1,0:T(8,128)(2,1)S(1)} %collective-permute-done.8), channel_id=1, source_target_pairs={{0,30},{2,0},{4,2},{6,4},{8,6},{10,8},{12,10},{14,12},{16,14},{18,... | collective-permute-start | bytes 393224 | tf_op jit(solution)/shard_map/ppermute | solution.py:20
  469.3 6.1 collective-permute-done.9
  475.4 6.1 collective-permute-start.10
  481.5 5.2 collective-permute-done.10
  486.6 6.1 collective-permute-start.11
  493.9 1.3 collective-permute-done.11
  495.2 6.1 collective-permute-start.12
  501.4 1.7 collective-permute-done.5
  504.1 5.9 collective-permute-start.13
  509.9 1.7 collective-permute-done.6
  511.9 2.3 collective-permute-done.13
  514.2 4.3 collective-permute-start.14
  518.5 1.8 collective-permute-done.7
  522.3 3.1 fusion.28
  525.4 50.5 %all-gather.14.cloned.1.call-done = bf16[2048,512]{1,0:T(8,128)(2,1)} async-done(((bf16[128,512]{1,0:T(8,128)(2,1)}), bf16[2048,512]{1,0:T(8,128)(2,1)}) %all-gather.14.cloned.1.call-update) | async-done | bytes 2097168 | tf_op jit(solution)/shard_map/all_gather | solution.py:94
  575.9 4.1 convolution_convert_fusion.1
  580.0 16.1 %gather_fusion.1 = bf16[1536,2048]{1,0:T(8,128)(2,1)} fusion(bf16[1280,2048]{1,0:T(8,128)(2,1)} %bitcast.10, s32[2048]{0:T(1024)S(1)} %pad_clamp_fusion.1), kind=kCustom, calls=%fused_computation.1 | custom fusion | bytes 12589056 | tf_op jit(solution)/shard_map/gather | solution.py:129
  596.1 11.7 %reshape.194 = f32[256,6,2048]{2,1,0:T(8,128)} reshape(bf16[1536,2048]{1,0:T(8,128)(2,1)} %gather_fusion.1) | data formatting | bytes 18874368 | tf_op jit(solution)/shard_map/convert_element_type | solution.py:129
  607.8 9.5 %multiply_reduce_fusion = f32[256,2048]{1,0:T(8,128)S(1)} fusion(f32[256,6,2048]{2,1,0:T(8,128)} %reshape.194, f32[256,6]{1,0:T(8,128)S(1)} %copy.36), kind=kLoop, calls=%fused_computation.3 | loop fusion | flops 5767168 | bytes 14686208 | tf_op jit(solution)/shard_map/reduce_sum | solution.py:131
  618.6 7.3 %reduce-scatter.2.cloned.1.call-done = bf16[256,1024]{1,0:T(8,128)(2,1)} async-done(((bf16[256,2048]{1,0:T(8,128)(2,1)}), bf16[256,1024]{1,0:T(8,128)(2,1)}) %reduce-scatter.2.cloned.1.call-update) | async-done | bytes 524304 | tf_op jit(solution)/shard_map/reduce_scatter | solution.py:133
  625.9 1.3 copy.78
  629.6 3.2 copy.80
  632.8 1.3 copy.81
  (122 shorter events, 14.6 us)
Async XLA Ops:
  71.2 46.5 %all-to-all-start.2 = ((bf16[16,128,512]{2,1,0:T(8,128)(2,1)}), bf16[16,128,512]{2,1,0:T(8,128)(2,1)S(1)}, u32[]{:S(2)}, u32[]{:S(2)}) async-start(bf16[16,128,512]{2,1,0:T(8,128)(2,1)} %get-tuple-element.11), calls=%async_computation.2 | async-start | bytes 4194304 | tf_op jit(solution)/shard_map/all_to_all | solution.py:66
  75.1 52.4 %copy-start.13 = (s32[256,6]{0,1:T(8,128)S(1)}, s32[256,6]{0,1:T(8,128)}, u32[]{:S(2)}) copy-start(s32[256,6]{0,1:T(8,128)} %param.11) | copy-start | bytes 18436
  78.9 54.5 %copy-start.3 = (bf16[256,2048]{1,0:T(8,128)(2,1)S(1)}, bf16[256,2048]{1,0:T(8,128)(2,1)}, u32[]{:S(2)}) copy-start(bf16[256,2048]{1,0:T(8,128)(2,1)} %param.10) | copy-start | bytes 3145732
  117.7 16.3 %copy-start.1 = (bf16[16,128,512]{2,1,0:T(8,128)(2,1)}, bf16[16,128,512]{2,1,0:T(8,128)(2,1)S(1)}, u32[]{:S(2)}) copy-start(bf16[16,128,512]{2,1,0:T(8,128)(2,1)S(1)} %all-to-all-done.2) | copy-start | bytes 6291460
  117.7 52.5 %all-to-all-start.3 = ((bf16[16,128,512]{2,1,0:T(8,128)(2,1)}), bf16[16,128,512]{2,1,0:T(8,128)(2,1)}, u32[]{:S(2)}, u32[]{:S(2)}) async-start(bf16[16,128,512]{2,1,0:T(8,128)(2,1)} %convert_element_type.70), calls=%async_computation.3 | async-start | bytes 4194304 | tf_op jit(solution)/shard_map/all_to_all | solution.py:67
  134.0 1.0 copy-start.4
  170.2 107.1 %all-to-all-start = ((bf16[16,80,2048]{2,1,0:T(8,128)(2,1)}), bf16[16,80,2048]{2,1,0:T(8,128)(2,1)}, u32[]{:S(2)}, u32[]{:S(2)}) async-start(bf16[16,80,2048]{2,1,0:T(8,128)(2,1)} %constant_dynamic-slice_fusion.1), calls=%async_computation | async-start | bytes 10485760 | tf_op jit(solution)/shard_map/all_to_all | solution.py:109
  180.0 17.3 %all-gather.6.cloned.1.call-start = ((), (), s32[]{:S(2)}) async-start(), calls=%async_computation.6 | async-start | bytes 6291456 | tf_op jit(solution)/shard_map/all_gather | solution.py:104
  180.7 107.1 %all-gather.8.cloned.1.call-start = ((), (), s32[]{:S(2)}) async-start(), calls=%async_computation.7 | async-start | bytes 6291456 | tf_op jit(solution)/shard_map/all_gather | solution.py:105
  181.5 116.9 %all-gather.10.cloned.1.call-start = ((), (), s32[]{:S(2)}) async-start(), calls=%async_computation.8 | async-start | bytes 6291456 | tf_op jit(solution)/shard_map/all_gather | solution.py:106
  320.2 24.3 %copy-start.11 = (f32[128,512]{1,0:T(8,128)S(1)}, f32[128,512]{1,0:T(8,128)}, u32[]{:S(2)}) copy-start(f32[128,512]{1,0:T(8,128)} %param.17) | copy-start | bytes 786436
  320.2 24.4 %copy-start.12 = (f32[128,512]{1,0:T(8,128)S(1)}, f32[128,512]{1,0:T(8,128)}, u32[]{:S(2)}) copy-start(f32[128,512]{1,0:T(8,128)} %param.18) | copy-start | bytes 786436
  320.2 24.4 %copy-start.15 = (f32[128]{0:T(128)S(1)}, f32[128]{0:T(128)}, u32[]{:S(2)}) copy-start(f32[128]{0:T(128)} %param.13) | copy-start | bytes 1540
  320.2 182.9 %copy-start.10 = (f32[128,512]{1,0:T(8,128)S(1)}, f32[128,512]{1,0:T(8,128)}, u32[]{:S(2)}) copy-start(f32[128,512]{1,0:T(8,128)} %param.19) | copy-start | bytes 786436
  320.2 191.5 %copy-start.14 = (f32[256,6]{0,1:T(8,128)S(1)}, f32[256,6]{0,1:T(8,128)}, u32[]{:S(2)}) copy-start(f32[256,6]{0,1:T(8,128)} %param.12) | copy-start | bytes 18436
  320.2 259.7 %all-to-all-start.4 = ((bf16[16,80,2048]{2,1,0:T(8,128)(2,1)}), bf16[16,80,2048]{2,1,0:T(8,128)(2,1)}, u32[]{:S(2)}, u32[]{:S(2)}) async-start(bf16[16,80,2048]{2,1,0:T(8,128)(2,1)} %bitcast.44), calls=%async_computation.4 | async-start | bytes 10485760 | tf_op jit(solution)/shard_map/all_to_all | solution.py:123
  344.5 177.0 %all-gather.12.cloned.1.call-start = ((), (), s32[]{:S(2)}) async-start(), calls=%async_computation.9 | async-start | bytes 2228224 | tf_op jit(solution)/shard_map/all_gather | solution.py:92
  345.4 230.5 %all-gather.14.cloned.1.call-start = ((), (), s32[]{:S(2)}) async-start(), calls=%async_computation.10 | async-start | bytes 2228224 | tf_op jit(solution)/shard_map/all_gather | solution.py:94
  345.4 101.2 %collective-permute-start = (bf16[128,512]{1,0:T(8,128)(2,1)S(1)}, bf16[128,512]{1,0:T(8,128)(2,1)S(1)}, u32[]{:S(2)}, u32[]{:S(2)}) collective-permute-start(bf16[128,512]{1,0:T(8,128)(2,1)S(1)} %get-tuple-element.10), channel_id=1, source_target_pairs={{0,2},{2,4},{4,6},{6,8},{8,10},{10,12},{12,14},{14,16},{16,18},{18... | collective-permute-start | bytes 393224 | tf_op jit(solution)/shard_map/ppermute | solution.py:16
  446.6 11.5 %collective-permute-start.1 = (bf16[128,512]{1,0:T(8,128)(2,1)S(1)}, bf16[128,512]{1,0:T(8,128)(2,1)S(1)}, u32[]{:S(2)}, u32[]{:S(2)}) collective-permute-start(bf16[128,512]{1,0:T(8,128)(2,1)S(1)} %collective-permute-done), channel_id=1, source_target_pairs={{0,2},{2,4},{4,6},{6,8},{8,10},{10,12},{12,14},{14,16},{16,18},{18... | collective-permute-start | bytes 393224 | tf_op jit(solution)/shard_map/ppermute | solution.py:16
  446.6 14.0 %collective-permute-start.8 = (bf16[128,512]{1,0:T(8,128)(2,1)S(1)}, bf16[128,512]{1,0:T(8,128)(2,1)S(1)}, u32[]{:S(2)}, u32[]{:S(2)}) collective-permute-start(bf16[128,512]{1,0:T(8,128)(2,1)S(1)} %get-tuple-element.10), channel_id=1, source_target_pairs={{0,30},{2,0},{4,2},{6,4},{8,6},{10,8},{12,10},{14,12},{16,14},{18,... | collective-permute-start | bytes 393224 | tf_op jit(solution)/shard_map/ppermute | solution.py:20
  458.1 11.1 %collective-permute-start.2 = (bf16[128,512]{1,0:T(8,128)(2,1)S(1)}, bf16[128,512]{1,0:T(8,128)(2,1)S(1)}, u32[]{:S(2)}, u32[]{:S(2)}) collective-permute-start(bf16[128,512]{1,0:T(8,128)(2,1)S(1)} %collective-permute-done.1), channel_id=1, source_target_pairs={{0,2},{2,4},{4,6},{6,8},{8,10},{10,12},{12,14},{14,16},{16,18},{18... | collective-permute-start | bytes 393224 | tf_op jit(solution)/shard_map/ppermute | solution.py:16
  460.6 14.8 %collective-permute-start.9 = (bf16[128,512]{1,0:T(8,128)(2,1)S(1)}, bf16[128,512]{1,0:T(8,128)(2,1)S(1)}, u32[]{:S(2)}, u32[]{:S(2)}) collective-permute-start(bf16[128,512]{1,0:T(8,128)(2,1)S(1)} %collective-permute-done.8), channel_id=1, source_target_pairs={{0,30},{2,0},{4,2},{6,4},{8,6},{10,8},{12,10},{14,12},{16,14},{18,... | collective-permute-start | bytes 393224 | tf_op jit(solution)/shard_map/ppermute | solution.py:20
  469.3 12.2 %collective-permute-start.3 = (bf16[128,512]{1,0:T(8,128)(2,1)S(1)}, bf16[128,512]{1,0:T(8,128)(2,1)S(1)}, u32[]{:S(2)}, u32[]{:S(2)}) collective-permute-start(bf16[128,512]{1,0:T(8,128)(2,1)S(1)} %collective-permute-done.2), channel_id=1, source_target_pairs={{0,2},{2,4},{4,6},{6,8},{8,10},{10,12},{12,14},{14,16},{16,18},{18... | collective-permute-start | bytes 393224 | tf_op jit(solution)/shard_map/ppermute | solution.py:16
  475.4 11.2 %collective-permute-start.10 = (bf16[128,512]{1,0:T(8,128)(2,1)S(1)}, bf16[128,512]{1,0:T(8,128)(2,1)S(1)}, u32[]{:S(2)}, u32[]{:S(2)}) collective-permute-start(bf16[128,512]{1,0:T(8,128)(2,1)S(1)} %collective-permute-done.9), channel_id=1, source_target_pairs={{0,30},{2,0},{4,2},{6,4},{8,6},{10,8},{12,10},{14,12},{16,14},{18,... | collective-permute-start | bytes 393224 | tf_op jit(solution)/shard_map/ppermute | solution.py:20
  481.5 12.4 %collective-permute-start.4 = (bf16[128,512]{1,0:T(8,128)(2,1)S(1)}, bf16[128,512]{1,0:T(8,128)(2,1)S(1)}, u32[]{:S(2)}, u32[]{:S(2)}) collective-permute-start(bf16[128,512]{1,0:T(8,128)(2,1)S(1)} %collective-permute-done.3), channel_id=1, source_target_pairs={{0,2},{2,4},{4,6},{6,8},{8,10},{10,12},{12,14},{14,16},{16,18},{18... | collective-permute-start | bytes 393224 | tf_op jit(solution)/shard_map/ppermute | solution.py:16
  486.6 8.6 %collective-permute-start.11 = (bf16[128,512]{1,0:T(8,128)(2,1)S(1)}, bf16[128,512]{1,0:T(8,128)(2,1)S(1)}, u32[]{:S(2)}, u32[]{:S(2)}) collective-permute-start(bf16[128,512]{1,0:T(8,128)(2,1)S(1)} %collective-permute-done.10), channel_id=1, source_target_pairs={{0,30},{2,0},{4,2},{6,4},{8,6},{10,8},{12,10},{14,12},{16,14},{18,... | collective-permute-start | bytes 393224 | tf_op jit(solution)/shard_map/ppermute | solution.py:20
  493.9 9.2 %collective-permute-start.5 = (bf16[128,512]{1,0:T(8,128)(2,1)S(1)}, bf16[128,512]{1,0:T(8,128)(2,1)S(1)}, u32[]{:S(2)}, u32[]{:S(2)}) collective-permute-start(bf16[128,512]{1,0:T(8,128)(2,1)S(1)} %collective-permute-done.4), channel_id=1, source_target_pairs={{0,2},{2,4},{4,6},{6,8},{8,10},{10,12},{12,14},{14,16},{16,18},{18... | collective-permute-start | bytes 393224 | tf_op jit(solution)/shard_map/ppermute | solution.py:16
  495.2 8.9 %collective-permute-start.12 = (bf16[128,512]{1,0:T(8,128)(2,1)S(1)}, bf16[128,512]{1,0:T(8,128)(2,1)S(1)}, u32[]{:S(2)}, u32[]{:S(2)}) collective-permute-start(bf16[128,512]{1,0:T(8,128)(2,1)S(1)} %collective-permute-done.11), channel_id=1, source_target_pairs={{0,30},{2,0},{4,2},{6,4},{8,6},{10,8},{12,10},{14,12},{16,14},{18,... | collective-permute-start | bytes 393224 | tf_op jit(solution)/shard_map/ppermute | solution.py:20
  503.1 8.6 %collective-permute-start.6 = (bf16[128,512]{1,0:T(8,128)(2,1)S(1)}, bf16[128,512]{1,0:T(8,128)(2,1)S(1)}, u32[]{:S(2)}, u32[]{:S(2)}) collective-permute-start(bf16[128,512]{1,0:T(8,128)(2,1)S(1)} %collective-permute-done.5), channel_id=1, source_target_pairs={{0,2},{2,4},{4,6},{6,8},{8,10},{10,12},{12,14},{14,16},{16,18},{18... | collective-permute-start | bytes 393224 | tf_op jit(solution)/shard_map/ppermute | solution.py:16
  503.8 122.1 %reduce-scatter.2.cloned.1.call-start = ((), (), s32[]{:S(2)}) async-start(), calls=%async_computation.11 | async-start | bytes 1572864 | tf_op jit(solution)/shard_map/reduce_scatter | solution.py:133
  504.1 10.1 %collective-permute-start.13 = (bf16[128,512]{1,0:T(8,128)(2,1)S(1)}, bf16[128,512]{1,0:T(8,128)(2,1)S(1)}, u32[]{:S(2)}, u32[]{:S(2)}) collective-permute-start(bf16[128,512]{1,0:T(8,128)(2,1)S(1)} %collective-permute-done.12), channel_id=1, source_target_pairs={{0,30},{2,0},{4,2},{6,4},{8,6},{10,8},{12,10},{14,12},{16,14},{18,... | collective-permute-start | bytes 393224 | tf_op jit(solution)/shard_map/ppermute | solution.py:20
  511.7 8.7 %collective-permute-start.7 = (bf16[128,512]{1,0:T(8,128)(2,1)S(1)}, bf16[128,512]{1,0:T(8,128)(2,1)S(1)}, u32[]{:S(2)}, u32[]{:S(2)}) collective-permute-start(bf16[128,512]{1,0:T(8,128)(2,1)S(1)} %collective-permute-done.6), channel_id=1, source_target_pairs={{0,2},{2,4},{4,6},{6,8},{8,10},{10,12},{12,14},{14,16},{16,18},{18... | collective-permute-start | bytes 393224 | tf_op jit(solution)/shard_map/ppermute | solution.py:16
  514.2 6.8 %collective-permute-start.14 = (bf16[128,512]{1,0:T(8,128)(2,1)S(1)}, bf16[128,512]{1,0:T(8,128)(2,1)S(1)}, u32[]{:S(2)}, u32[]{:S(2)}) collective-permute-start(bf16[128,512]{1,0:T(8,128)(2,1)S(1)} %collective-permute-done.13), channel_id=1, source_target_pairs={{0,30},{2,0},{4,2},{6,4},{8,6},{10,8},{12,10},{14,12},{16,14},{18,... | collective-permute-start | bytes 393224 | tf_op jit(solution)/shard_map/ppermute | solution.py:20
  521.0 1.2 copy-start.5
  521.5 58.5 %copy-start.8 = (bf16[2048,512]{1,0:T(8,128)(2,1)}, bf16[2048,512]{1,0:T(8,128)(2,1)S(1)}, u32[]{:S(2)}) copy-start(bf16[2048,512]{1,0:T(8,128)(2,1)S(1)} %constant_dynamic-slice_fusion) | copy-start | bytes 6291460
  607.8 9.5 %copy-start.9 = (bf16[256,2048]{1,0:T(8,128)(2,1)S(1)}, bf16[256,2048]{1,0:T(8,128)(2,1)}, u32[]{:S(2)}) copy-start(bf16[256,2048]{1,0:T(8,128)(2,1)} %convolution_convert_fusion.1) | copy-start | bytes 3145732
  617.3 8.6 %copy-start = (bf16[16,128,512]{2,1,0:T(8,128)(2,1)S(1)}, bf16[16,128,512]{2,1,0:T(8,128)(2,1)}, u32[]{:S(2)}) copy-start(bf16[16,128,512]{2,1,0:T(8,128)(2,1)} %all_to_all.46) | copy-start | bytes 6291460
  625.9 2.3 copy-start.2
  628.3 4.5 copy-start.6
  629.6 4.5 copy-start.7
Sparse Core Ops, SparseCore 0:
  182.3 14.8 all-gather.5
  199.4 14.8 all-gather.7
  216.4 14.8 all-gather.9
  618.7 7.1 reduce-scatter.1
Sparse Core Ops, SparseCore 1:
  348.3 142.1 all-gather.11
  503.9 71.9 all-gather.13
